TPU v7x, 32 devices: a whole 2x2x4 slice. The times are simulated.
32 devices in a mesh: kv: 8 (over z, y), tp: 4 (over x, core).
Axes of the slice: x: 2, y: 2, z: 4, core: 2. Of those that a mesh axis runs over, the one named last changes fastest.
Arguments:
- tokens: bfloat16 [32, 4096], P(None, ('kv', 'tp')), may hold values from -12 to 12
- first_gain: bfloat16 [4096], replicated, may hold values from 0.099609375 to 1.8984375
- first_gate: bfloat16 [4096, 11264], P(None, ('kv', 'tp')), may hold values from -0.09375 to 0.09375
- first_up: bfloat16 [4096, 11264], P(None, ('kv', 'tp')), may hold values from -0.09375 to 0.09375
- first_down: bfloat16 [11264, 4096], P(('kv', 'tp')), may hold values from -0.109375 to 0.109375
- mix_gain: bfloat16 [4096], replicated, may hold values from 0.099609375 to 1.8984375
- query_weight: bfloat16 [4096, 1024], P('kv', 'tp'), may hold values from -0.09375 to 0.09375
- key_weight: bfloat16 [4096, 1024], P('kv', 'tp'), may hold values from -0.09375 to 0.09375
- value_weight: bfloat16 [4096, 2048], P('kv', 'tp'), may hold values from -0.09375 to 0.09375
- outgate_weight: bfloat16 [4096, 2048], P('kv', 'tp'), may hold values from -0.09375 to 0.09375
- ingate_weight: bfloat16 [4096, 8], P('kv'), may hold values from -0.09375 to 0.09375
- forget_weight: bfloat16 [4096, 8], P('kv'), may hold values from -0.09375 to 0.09375
- forget_bias: float32 [8], P('tp'), may hold values from -1 to 4
- head_gain: bfloat16 [2048], P('tp'), may hold values from 0.099609375 to 1.8984375
- mixout_weight: bfloat16 [2048, 4096], P('tp', 'kv'), may hold values from -0.125 to 0.125
- memory: float32 [32, 8, 128, 256], P('kv', 'tp'), may hold values from -0.6 to 0.6
- stabilizer: float32 [32, 8], P('kv', 'tp'), may hold values from -4 to 4
- second_gain: bfloat16 [4096], replicated, may hold values from 0.099609375 to 1.8984375
- second_gate: bfloat16 [4096, 11264], P(None, ('kv', 'tp')), may hold values from -0.09375 to 0.09375
- second_up: bfloat16 [4096, 11264], P(None, ('kv', 'tp')), may hold values from -0.09375 to 0.09375
- second_down: bfloat16 [11264, 4096], P(('kv', 'tp')), may hold values from -0.109375 to 0.109375
Outputs:
- layer_out: bfloat16 [32, 4096], P(None, ('kv', 'tp'))
- memory_next: float32 [32, 8, 128, 256], P('kv', 'tp')
- stabilizer_next: float32 [32, 8], P('kv', 'tp')
All inputs are finite; a program needn't handle non-finite values.
Results may differ from a plain program's by a relative error of at most 0.013.
Values may be sent and summed in bfloat16 or wider, within the bound.
A program may use at most 64 MiB of HBM per device.

v0:
```python
import jax
import jax.numpy as jnp
from jax import lax
from jax.sharding import PartitionSpec as P

epsilon = 1e-06


def row_scale(squares, model_width):
    return lax.rsqrt(squares / model_width + epsilon)[:, None]


def fold_columns(column_block, gain_vector, matrices):
    wide_block = column_block.astype(jnp.float32)
    gain_piece = gain_vector.astype(jnp.float32)
    normed = (wide_block * gain_piece).astype(jnp.bfloat16)
    updated = tuple(
        (jnp.dot(normed, matrix, preferred_element_type=jnp.float32) for matrix in matrices)
    )
    return (updated, jnp.sum(wide_block * wide_block, axis=1))


def half_mlp(tokens, norm_gain, gate_weight, up_weight, down_weight):
    model_width = norm_gain.shape[0]
    (gate_sum, up_sum), squares = fold_columns(
        lax.all_gather(tokens, ("kv", "tp"), axis=1, tiled=True),
        norm_gain,
        (gate_weight, up_weight),
    )
    row_factor = row_scale(squares, model_width)
    hidden = (jax.nn.silu(row_factor * gate_sum) * (row_factor * up_sum)).astype(jnp.bfloat16)
    branch = lax.psum_scatter(
        lax.dot_general(
            down_weight, hidden, (((0,), (1,)), ((), ())), preferred_element_type=jnp.float32
        ),
        ("kv", "tp"),
        scatter_dimension=0,
        tiled=True,
    ).T
    return (tokens.astype(jnp.float32) + 0.5 * branch).astype(jnp.bfloat16)


def on_device(
    tokens,
    first_gain,
    first_gate,
    first_up,
    first_down,
    mix_gain,
    query_weight,
    key_weight,
    value_weight,
    outgate_weight,
    ingate_weight,
    forget_weight,
    forget_bias,
    head_gain,
    mixout_weight,
    memory,
    stabilizer,
    second_gain,
    second_gate,
    second_up,
    second_down,
):
    first = half_mlp(tokens, first_gain, first_gate, first_up, first_down)
    matrices = (
        query_weight,
        key_weight,
        value_weight,
        outgate_weight,
        ingate_weight,
        forget_weight,
    )
    block_width = query_weight.shape[0]
    gain_block = lax.dynamic_slice_in_dim(
        mix_gain, lax.axis_index("kv") * block_width, block_width, 0
    )
    mix_partials, squares = fold_columns(
        lax.all_gather(first, "tp", axis=1, tiled=True), gain_block, matrices
    )
    query_sum, key_sum, value_sum, outgate_sum, ingate_sum, forget_sum, squares = (
        lax.psum_scatter(mix_partials[0], "kv", scatter_dimension=0, tiled=True),
        lax.psum_scatter(mix_partials[1], "kv", scatter_dimension=0, tiled=True),
        lax.psum_scatter(mix_partials[2], "kv", scatter_dimension=0, tiled=True),
        lax.psum_scatter(mix_partials[3], "kv", scatter_dimension=0, tiled=True),
        lax.psum_scatter(mix_partials[4], "kv", scatter_dimension=0, tiled=True),
        lax.psum_scatter(mix_partials[5], "kv", scatter_dimension=0, tiled=True),
        lax.psum_scatter(squares, "kv", scatter_dimension=0, tiled=True),
    )
    row_factor = row_scale(squares, mix_gain.shape[0])
    seq_local, heads_local, key_width, value_width = memory.shape
    query = (row_factor * query_sum).astype(jnp.bfloat16).reshape(seq_local, heads_local, key_width)
    keys = (row_factor * key_sum).astype(jnp.bfloat16).reshape(seq_local, heads_local, key_width)
    values = (
        (row_factor * value_sum).astype(jnp.bfloat16).reshape(seq_local, heads_local, value_width)
    )
    outgate = (
        (row_factor * outgate_sum).astype(jnp.bfloat16).reshape(seq_local, heads_local, value_width)
    )
    head_start = lax.axis_index("tp") * heads_local
    ingate = lax.dynamic_slice_in_dim(row_factor * ingate_sum, head_start, heads_local, 1)
    forget = (
        lax.dynamic_slice_in_dim(row_factor * forget_sum, head_start, heads_local, 1)
        + forget_bias[None, :]
    )
    log_forget = jax.nn.log_sigmoid(forget)
    ceiling = jnp.maximum(log_forget + stabilizer, ingate)
    retain = jnp.exp(log_forget + stabilizer - ceiling)
    admission = jnp.exp(ingate - ceiling)
    scaled_keys = keys.astype(jnp.float32) * key_width ** (-0.5)
    outer_product = jnp.einsum("shd,she->shde", scaled_keys, values.astype(jnp.float32))
    memory_next = retain[..., None, None] * memory + admission[..., None, None] * outer_product
    readout = jnp.einsum(
        "shd,shde->she", query.astype(jnp.float32), memory_next, precision=lax.Precision.HIGHEST
    )
    normalized = readout * lax.rsqrt(jnp.mean(readout * readout, axis=-1, keepdims=True) + epsilon)
    gated = (
        normalized
        * head_gain.reshape(heads_local, value_width).astype(jnp.float32)
        * jax.nn.sigmoid(outgate.astype(jnp.float32))
    )
    mixed = gated.reshape(seq_local, heads_local * value_width).astype(jnp.bfloat16)
    mix_terms = jnp.dot(
        lax.all_gather(mixed, "kv", axis=0, tiled=True),
        mixout_weight,
        preferred_element_type=jnp.float32,
    )
    mix_branch = lax.psum_scatter(
        mix_terms.astype(jnp.bfloat16), "tp", scatter_dimension=1, tiled=True
    ).astype(jnp.float32)
    after_mix = (first.astype(jnp.float32) + mix_branch).astype(jnp.bfloat16)
    layer_out = half_mlp(after_mix, second_gain, second_gate, second_up, second_down)
    return (layer_out, memory_next, ceiling)


def solution(mesh):
    in_specs = (
        P(None, ("kv", "tp")),
        P(),
        P(None, ("kv", "tp")),
        P(None, ("kv", "tp")),
        P(("kv", "tp"), None),
        P(),
        P("kv", "tp"),
        P("kv", "tp"),
        P("kv", "tp"),
        P("kv", "tp"),
        P("kv", None),
        P("kv", None),
        P("tp"),
        P("tp"),
        P("tp", "kv"),
        P("kv", "tp", None, None),
        P("kv", "tp"),
        P(),
        P(None, ("kv", "tp")),
        P(None, ("kv", "tp")),
        P(("kv", "tp"), None),
    )
    out_specs = (P(None, ("kv", "tp")), P("kv", "tp", None, None), P("kv", "tp"))
    return jax.shard_map(
        on_device, mesh=mesh, in_specs=in_specs, out_specs=out_specs, check_vma=False
    )
```

profile of v0, /device:TPU:0, one launch (start us, length us, event | category | flops | bytes accessed | tf_op | source)
XLA Modules:
  0.0 592.3 jit_solution(15332073534694084184)
XLA Ops:
  7.2 0.9 convert_element_type.97
  8.1 44.2 %all_gather.12 = bf16[32,4096]{1,0:T(8,128)(2,1)S(1)} all-gather(bf16[32,128]{1,0:T(8,128)(2,1)} %param.21), channel_id=1, replica_groups=mesh['kv'=8,'tp'=4] {'kv','tp'}, dimensions={1}, use_global_device_ids=true | all-gather | bytes 270336 | tf_op jit(solution)/shard_map/all_gather | solution.py:26
  52.4 2.7 convolution_multiply_fusion.3
  55.3 4.6 convolution_bitcast_fusion.1
  61.4 0.8 dynamic-slice_convert_fusion
  62.1 129.9 %reduce-scatter.6.cloned.1.call-done = f32[128,32]{0,1:T(8,128)} async-done(((f32[4096,32]{0,1:T(8,128)}), f32[128,32]{0,1:T(8,128)}) %reduce-scatter.6.cloned.1.call-update) | async-done | bytes 16400 | tf_op jit(solution)/shard_map/reduce_scatter | solution.py:32
  192.0 0.7 fusion.31
  192.7 5.2 all_gather.13
  198.5 0.7 fusion.40
  199.3 0.7 fusion.38
  200.0 1.7 fusion.36
  201.7 1.7 fusion.42
  203.4 1.9 fusion.34
  205.4 1.9 fusion.32
  207.3 65.3 %all-reduce.12.cloned.1.call-done = (f32[32]{0:T(128)}, f32[32,256]{1,0:T(8,128)}, f32[32,256]{1,0:T(8,128)}, f32[32,8]{1,0:T(8,128)}, f32[32,8]{1,0:T(8,128)}) async-done(((f32[32]{0:T(128)}, f32[32,256]{1,0:T(8,128)}, f32[32,256]{1,0:T(8,128)}, f32[32,8]{1,0:T(8,128)}, f32[32,8]{1,0:T(8,128)}), (f32[32]{0:T(128)}, f32[32,256]{1,0:T(8,128)}, f32[32,256]{1,0:T(8,128)}, f32[32,8]{1,0:T(8,128)}, ...) | async-done | bytes 67728
  272.6 0.8 fusion.56
  273.3 0.8 convert_multiply_fusion.6
  274.1 0.8 dynamic-slice_multiply_fusion.4
  275.1 72.3 %all-reduce.14.cloned.1.call-done = (f32[32,512]{1,0:T(8,128)}, f32[32,512]{1,0:T(8,128)}) async-done(((f32[32,512]{1,0:T(8,128)}, f32[32,512]{1,0:T(8,128)}), (f32[32,512]{1,0:T(8,128)}, f32[32,512]{1,0:T(8,128)})) %all-reduce.14.cloned.1.call-update) | async-done | bytes 131088
  347.4 0.8 fusion.50
  348.2 1.5 multiply_add_fusion
  349.7 1.0 copy-done.1
  351.3 30.6 %all-gather = bf16[8,4,512]{2,1,0:T(4,128)(2,1)S(1)} all-gather(bf16[1,4,512]{2,1,0:T(4,128)(2,1)S(1)} %reshape.65), channel_id=1, replica_groups=mesh['kv'=8,'tp'=4] {'kv'}, dimensions={0}, use_global_device_ids=true | all-gather | bytes 36864 | tf_op jit(solution)/shard_map/all_gather | solution.py:125
  382.1 0.8 copy.30
  383.0 18.8 %reduce-scatter.10.cloned.1.call-done = bf16[128,32]{1,0:T(8,128)(2,1)} async-done(((bf16[512,32]{1,0:T(8,128)(2,1)}), bf16[128,32]{1,0:T(8,128)(2,1)}) %reduce-scatter.10.cloned.1.call-update) | async-done | bytes 8208
  401.8 0.8 copy.31
  402.7 41.3 %all_gather.15 = bf16[32,4096]{1,0:T(8,128)(2,1)S(1)} all-gather(bf16[32,128]{1,0:T(8,128)(2,1)S(1)} %add_convert_fusion), channel_id=1, replica_groups=mesh['kv'=8,'tp'=4] {'kv','tp'}, dimensions={1}, use_global_device_ids=true | all-gather | bytes 270336 | tf_op jit(solution)/shard_map/all_gather | solution.py:26
  444.2 2.7 convolution_multiply_fusion.1
  446.9 5.5 convolution_bitcast_fusion
  452.4 0.6 copy.27
  453.1 131.4 %reduce-scatter.8.cloned.1.call-done = f32[128,32]{0,1:T(8,128)} async-done(((f32[4096,32]{0,1:T(8,128)}), f32[128,32]{0,1:T(8,128)}) %reduce-scatter.8.cloned.1.call-update) | async-done | bytes 16400 | tf_op jit(solution)/shard_map/reduce_scatter | solution.py:32
  584.5 1.3 fusion.30
  (54 shorter events, 3.1 us)
Async XLA Ops:
  7.2 48.0 %copy-start = (bf16[352,4096]{1,0:T(8,128)(2,1)S(1)}, bf16[352,4096]{1,0:T(8,128)(2,1)}, u32[]{:S(2)}) copy-start(bf16[352,4096]{1,0:T(8,128)(2,1)} %param.25) | copy-start | bytes 8650756
  7.2 184.8 %reduce-scatter.6.cloned.1.call-start = ((), (), s32[]{:S(2)}) async-start(), calls=%async_computation.3 | async-start | bytes 540672 | tf_op jit(solution)/shard_map/reduce_scatter | solution.py:32
  55.2 4.8 copy-start.7
  55.2 4.8 copy-start.8
  55.2 4.9 copy-start.10
  55.2 136.8 %copy-start.3 = (bf16[32,128]{1,0:T(8,128)(2,1)S(1)}, bf16[32,128]{1,0:T(8,128)(2,1)}, u32[]{:S(2)}) copy-start(bf16[32,128]{1,0:T(8,128)(2,1)} %param.21) | copy-start | bytes 24580
  55.2 143.3 %copy-start.5 = (bf16[512,8]{0,1:T(8,128)(2,1)S(1)}, bf16[512,8]{0,1:T(8,128)(2,1)}, u32[]{:S(2)}) copy-start(bf16[512,8]{0,1:T(8,128)(2,1)} %param.32) | copy-start | bytes 24580
  55.3 144.0 %copy-start.6 = (bf16[512,8]{0,1:T(8,128)(2,1)S(1)}, bf16[512,8]{0,1:T(8,128)(2,1)}, u32[]{:S(2)}) copy-start(bf16[512,8]{0,1:T(8,128)(2,1)} %param.31) | copy-start | bytes 24580
  59.9 215.0 %copy-start.9 = (f32[2]{0:T(128)S(1)}, f32[2]{0:T(128)}, u32[]{:S(2)}) copy-start(f32[2]{0:T(128)} %param.33) | copy-start | bytes 28
  59.9 212.6 %all-reduce.12.cloned.1.call-start = ((), (), s32[]{:S(2)}) async-start(), calls=%async_computation.6 | async-start | bytes 197632
  198.5 183.4 %copy-start.2 = (bf16[512,512]{1,0:T(8,128)(2,1)S(1)}, bf16[512,512]{1,0:T(8,128)(2,1)}, u32[]{:S(2)}) copy-start(bf16[512,512]{1,0:T(8,128)(2,1)} %param.35) | copy-start | bytes 1572868
  203.4 179.6 %copy-start.4 = (bf16[4096]{0:T(1024)(128)(2,1)S(1)}, bf16[4096]{0:T(1024)(128)(2,1)}, u32[]{:S(2)}) copy-start(bf16[4096]{0:T(1024)(128)(2,1)} %param.38) | copy-start | bytes 24580
  205.3 142.1 %all-reduce.14.cloned.1.call-start = ((), (), s32[]{:S(2)}) async-start(), calls=%async_computation.7 | async-start | bytes 262144
  207.3 194.6 %reduce-scatter.10.cloned.1.call-start = ((), (), s32[]{:S(2)}) async-start(), calls=%async_computation.5 | async-start | bytes 163840
  349.7 1.0 copy-start.1
  382.9 201.5 %reduce-scatter.8.cloned.1.call-start = ((), (), s32[]{:S(2)}) async-start(), calls=%async_computation.4 | async-start | bytes 540672 | tf_op jit(solution)/shard_map/reduce_scatter | solution.py:32
Sparse Core Ops, SparseCore 0:
  60.1 131.9 reduce-scatter.5
  205.4 67.0 all-reduce.11
  276.6 70.7 all-reduce.13
  383.1 18.7 reduce-scatter.9
  452.6 131.8 reduce-scatter.7
where the time goes:
time: 593 us; the launch traced here: 592 us
  waiting for transfers between devices  418 us (70%)
  blocking collectives  121 us (20%)
  matrix products  24.9 us (4%)
  between operations  14.6 us (2%)
  other arithmetic  9.58 us (2%)
    reduce_scatter x2, waiting for transfers between devices, half_mlp(): lax.psum_scatter(lax.dot_general(down_weight, hidden, (((0,), (1,)), ((),...  261 us
    unnamed x8, waiting for transfers between devices  156 us
    all_gather x2, blocking collectives, half_mlp(): lax.all_gather(tokens, ('kv', 'tp'), axis=1, tiled=True)  85.5 us
    all_gather x1, blocking collectives, on_device(): lax.all_gather(mixed, 'kv', axis=0, tiled=True)  30.6 us
    dot_general x8, matrix products, fold_columns(): jnp.dot(normed, matrix, preferred_element_type=jnp.float32)  14.1 us
  transfers between devices with their start and end apart: 5, of which 5 were waited for; matrix products, arithmetic and copies ran while one was open for 1% of the time, Pallas kernels for 0%

commit v1 on v0

--- a/solution.py
+++ b/solution.py
@@ -1,6 +1,10 @@
+import functools
+
 import jax
 import jax.numpy as jnp
 from jax import lax
+from jax.experimental import pallas as pl
+from jax.experimental.pallas import tpu as pltpu
 from jax.sharding import PartitionSpec as P
 
 epsilon = 1e-06
@@ -134,6 +138,571 @@
     return (layer_out, memory_next, ceiling)
 
 
+def fused_kernel(
+    kv_count,
+    tp_count,
+    tokens,
+    first_gain,
+    mix_gain,
+    second_gain,
+    head_gain,
+    forget_bias,
+    stabilizer,
+    first_gate,
+    first_up,
+    first_down,
+    query_weight,
+    key_weight,
+    value_weight,
+    outgate_weight,
+    ingate_weight,
+    forget_weight,
+    mixout_weight,
+    memory,
+    second_gate,
+    second_up,
+    second_down,
+    layer_out,
+    memory_next,
+    ceiling_out,
+    gate_a,
+    up_a,
+    down_a,
+    gate_b,
+    up_b,
+    down_b,
+    query_w,
+    key_w,
+    value_w,
+    outgate_w,
+    ingate_w,
+    forget_w,
+    mixout_w,
+    memory_v,
+    gathered_a,
+    parts_a,
+    landed_a,
+    gathered_b,
+    parts_b,
+    landed_b,
+    first_v,
+    block_v,
+    proj_send,
+    proj_land,
+    reduced,
+    readout_v,
+    mixed_send,
+    mixed_land,
+    mixed_all,
+    mix_send,
+    mix_land,
+    after_v,
+    load_sem,
+    store_sem,
+    all_send,
+    all_recv,
+    tp_send,
+    tp_recv,
+    kv_send,
+    kv_recv,
+):
+    total = kv_count * tp_count
+    my_kv = lax.axis_index("kv")
+    my_tp = lax.axis_index("tp")
+    me = my_kv * tp_count + my_tp
+    rows, chunk = tokens.shape
+    block = tp_count * chunk
+    model_width = total * chunk
+    seq_local, heads_local, key_width, value_width = memory.shape
+
+    loads = [
+        pltpu.make_async_copy(source, target, load_sem.at[n])
+        for n, (source, target) in enumerate(
+            (
+                (first_gate, gate_a),
+                (first_up, up_a),
+                (first_down, down_a),
+                (query_weight, query_w),
+                (key_weight, key_w),
+                (value_weight, value_w),
+                (outgate_weight, outgate_w),
+                (ingate_weight, ingate_w),
+                (forget_weight, forget_w),
+                (memory, memory_v),
+                (mixout_weight, mixout_w),
+                (second_gate, gate_b),
+                (second_up, up_b),
+                (second_down, down_b),
+            )
+        )
+    ]
+    for load in loads[:3]:
+        load.start()
+
+    barrier = pltpu.get_barrier_semaphore()
+
+    def greet(step, carry):
+        peer = (me + step) % total
+        pl.semaphore_signal(
+            barrier,
+            inc=1,
+            device_id={"kv": peer // tp_count, "tp": peer % tp_count},
+            device_id_type=pl.DeviceIdType.MESH,
+        )
+        return carry
+
+    lax.fori_loop(1, total, greet, 0)
+    pl.semaphore_wait(barrier, total - 1)
+
+    def send(source, target, send_sem, recv_sem, kv_index, tp_index):
+        return pltpu.make_async_remote_copy(
+            src_ref=source,
+            dst_ref=target,
+            send_sem=send_sem,
+            recv_sem=recv_sem,
+            device_id={"kv": kv_index, "tp": tp_index},
+            device_id_type=pl.DeviceIdType.MESH,
+        )
+
+    def share_all(source, target, phase):
+        def step_of(step, carry):
+            peer = (me + step) % total
+            send(
+                source,
+                target.at[me],
+                all_send.at[phase, peer],
+                all_recv.at[phase, me],
+                peer // tp_count,
+                peer % tp_count,
+            ).start()
+            return carry
+
+        lax.fori_loop(1, total, step_of, 0)
+
+    def sent_all(source_of, target, phase):
+        def step_of(step, carry):
+            peer = (me + step) % total
+            send(
+                source_of(peer),
+                target.at[me],
+                all_send.at[phase, peer],
+                all_recv.at[phase, me],
+                peer // tp_count,
+                peer % tp_count,
+            ).wait_send()
+            return carry
+
+        lax.fori_loop(1, total, step_of, 0)
+
+    def arrived(target, phase, peer):
+        send(
+            target.at[peer],
+            target.at[peer],
+            all_send.at[phase, peer],
+            all_recv.at[phase, peer],
+            peer // tp_count,
+            peer % tp_count,
+        ).wait_recv()
+
+    def half(own, gain, gate_w, up_w, down_w, gathered, parts, landed, phase, ready):
+        share_all(own, gathered, phase)
+        gathered[me] = own[...]
+        ready(0)
+        hidden_units = gate_w.shape[1]
+
+        def group_of(step, carry):
+            gate_sum, up_sum, squares = carry
+            group = (my_kv + step) % kv_count
+            for t in range(tp_count):
+                peer = group * tp_count + t
+
+                @pl.when(peer != me)
+                def _():
+                    arrived(gathered, phase, peer)
+
+            wide = jnp.concatenate(
+                [gathered[group * tp_count + t].astype(jnp.float32) for t in range(tp_count)],
+                axis=1,
+            )
+            start = pl.multiple_of(group * block, block)
+            normed = (wide * gain[:, pl.ds(start, block)].astype(jnp.float32)).astype(jnp.bfloat16)
+            gate_sum = gate_sum + jnp.dot(
+                normed, gate_w[pl.ds(start, block), :], preferred_element_type=jnp.float32
+            )
+            up_sum = up_sum + jnp.dot(
+                normed, up_w[pl.ds(start, block), :], preferred_element_type=jnp.float32
+            )
+            return gate_sum, up_sum, squares + jnp.sum(wide * wide, axis=1, keepdims=True)
+
+        zero = jnp.zeros((rows, hidden_units), jnp.float32)
+        gate_sum, up_sum, squares = lax.fori_loop(
+            0, kv_count, group_of, (zero, zero, jnp.zeros((rows, 1), jnp.float32))
+        )
+        factor = lax.rsqrt(squares / model_width + epsilon)
+        gate_sum = factor * gate_sum
+        hidden = (gate_sum / (1.0 + jnp.exp(-gate_sum)) * (factor * up_sum)).astype(jnp.bfloat16)
+        ready(1)
+
+        def ship(group):
+            for t in range(tp_count):
+                peer = group * tp_count + t
+
+                @pl.when(peer != me)
+                def _():
+                    send(
+                        parts.at[peer],
+                        landed.at[me],
+                        all_send.at[phase + 1, peer],
+                        all_recv.at[phase + 1, me],
+                        group,
+                        t,
+                    ).start()
+
+        def down_of(step, carry):
+            group = (my_kv + 1 + step) % kv_count
+            start = pl.multiple_of(group * block, block)
+            part = jnp.dot(
+                hidden, down_w[:, pl.ds(start, block)], preferred_element_type=jnp.float32
+            ).astype(jnp.bfloat16)
+            for t in range(tp_count):
+                parts[group * tp_count + t] = part[:, t * chunk : (t + 1) * chunk]
+
+            @pl.when(step > 0)
+            def _():
+                ship((my_kv + step) % kv_count)
+
+            return carry
+
+        lax.fori_loop(0, kv_count, down_of, 0)
+        ship(my_kv)
+
+        def add_of(step, carry):
+            peer = (me + step) % total
+            arrived(landed, phase + 1, peer)
+            return carry + landed[peer].astype(jnp.float32)
+
+        branch = lax.fori_loop(1, total, add_of, parts[me].astype(jnp.float32))
+        return (own[...].astype(jnp.float32) + 0.5 * branch).astype(jnp.bfloat16)
+
+    def ready_a(stage):
+        if stage == 0:
+            for load in loads[3:]:
+                load.start()
+            loads[0].wait()
+            loads[1].wait()
+            proj_send[...] = jnp.zeros_like(proj_send)
+            reduced[...] = jnp.zeros_like(reduced)
+            readout_v[...] = jnp.zeros_like(readout_v)
+        else:
+            loads[2].wait()
+
+    def ready_b(stage):
+        if stage == 0:
+            loads[11].wait()
+            loads[12].wait()
+        else:
+            loads[13].wait()
+
+    first = half(
+        tokens, first_gain, gate_a, up_a, down_a, gathered_a, parts_a, landed_a, 0, ready_a
+    )
+    first_v[...] = first
+
+    def tp_copy(source, target, phase, index):
+        return send(
+            source, target.at[my_tp], tp_send.at[phase, index], tp_recv.at[phase, my_tp], my_kv, index
+        )
+
+    def tp_arrived(target, phase, index):
+        send(
+            target.at[index],
+            target.at[index],
+            tp_send.at[phase, index],
+            tp_recv.at[phase, index],
+            my_kv,
+            index,
+        ).wait_recv()
+
+    def kv_copy(source, target, phase, index):
+        return send(
+            source, target.at[my_kv], kv_send.at[phase, index], kv_recv.at[phase, my_kv], index, my_tp
+        )
+
+    def kv_arrived(target, phase, index):
+        send(
+            target.at[index],
+            target.at[index],
+            kv_send.at[phase, index],
+            kv_recv.at[phase, index],
+            index,
+            my_tp,
+        ).wait_recv()
+
+    for step in range(1, tp_count):
+        tp_copy(first_v, block_v, 0, (my_tp + step) % tp_count).start()
+    block_v[my_tp] = first
+    for load in loads[3:9]:
+        load.wait()
+    for step in range(1, tp_count):
+        tp_arrived(block_v, 0, (my_tp + step) % tp_count)
+    wide = jnp.concatenate([block_v[t].astype(jnp.float32) for t in range(tp_count)], axis=1)
+    start = pl.multiple_of(my_kv * block, block)
+    normed = (wide * mix_gain[:, pl.ds(start, block)].astype(jnp.float32)).astype(jnp.bfloat16)
+    offsets = [0]
+    for weight in (query_w, key_w, value_w, outgate_w):
+        offsets.append(offsets[-1] + weight.shape[1])
+    edge = offsets[-1]
+    lane = 128
+    head_count = ingate_w.shape[1]
+    pieces = [
+        (offset, jnp.dot(normed, weight[...], preferred_element_type=jnp.float32))
+        for offset, weight in zip(
+            offsets[:4] + [edge, edge + lane],
+            (query_w, key_w, value_w, outgate_w, ingate_w, forget_w),
+        )
+    ]
+    squares = jnp.broadcast_to(jnp.sum(wide * wide, axis=1, keepdims=True), (rows, lane))
+    pieces.append((edge + 2 * lane, squares))
+    for k in range(kv_count):
+        for offset, piece in pieces:
+            proj_send[k, :, offset : offset + piece.shape[1]] = piece[
+                k * seq_local : (k + 1) * seq_local, :
+            ]
+    for step in range(1, kv_count):
+        peer = (my_kv + step) % kv_count
+        kv_copy(proj_send.at[peer], proj_land, 0, peer).start()
+    loads[9].wait()
+    summed = proj_send[my_kv]
+    for step in range(1, kv_count):
+        peer = (my_kv + step) % kv_count
+        kv_arrived(proj_land, 0, peer)
+        summed = summed + proj_land[peer]
+    reduced[0:seq_local, :] = summed
+    everything = reduced[...]
+    factor = lax.rsqrt(everything[:, edge + 2 * lane : edge + 2 * lane + 1] / model_width + epsilon)
+    query, keys, values, outgate = [
+        (factor * everything[:, offsets[n] : offsets[n + 1]]).astype(jnp.bfloat16).astype(jnp.float32)
+        for n in range(4)
+    ]
+    ingate_sum = everything[:, edge : edge + head_count]
+    forget_sum = everything[:, edge + lane : edge + lane + head_count]
+    ingate = ingate_sum[:, 0:heads_local]
+    forget = forget_sum[:, 0:heads_local]
+    for t in range(1, tp_count):
+        here = my_tp == t
+        ingate = jnp.where(here, ingate_sum[:, t * heads_local : (t + 1) * heads_local], ingate)
+        forget = jnp.where(here, forget_sum[:, t * heads_local : (t + 1) * heads_local], forget)
+    ingate = (factor * ingate)[0:seq_local]
+    forget = (factor * forget)[0:seq_local] + forget_bias[...]
+    log_forget = jnp.minimum(forget, 0.0) - jnp.log1p(jnp.exp(-jnp.abs(forget)))
+    shifted = log_forget + stabilizer[...]
+    ceiling = jnp.maximum(shifted, ingate)
+    retain = jnp.exp(shifted - ceiling)
+    admission = jnp.exp(ingate - ceiling) * key_width ** (-0.5)
+    ceiling_out[...] = ceiling
+    row_index = lax.broadcasted_iota(jnp.int32, (reduced.shape[0], key_width), 0)
+    stores = []
+    for h in range(heads_local):
+        head_keys = keys[:, h * key_width : (h + 1) * key_width]
+        head_values = values[:, h * value_width : (h + 1) * value_width]
+        head_query = query[:, h * key_width : (h + 1) * key_width]
+        for s in range(seq_local):
+            outer = lax.dot_general(
+                jnp.where(row_index == s, head_keys, 0.0),
+                head_values,
+                (((0,), (0,)), ((), ())),
+                preferred_element_type=jnp.float32,
+            )
+            updated = (
+                retain[s : s + 1, h : h + 1] * memory_v[s, h]
+                + admission[s : s + 1, h : h + 1] * outer
+            )
+            memory_v[s, h] = updated
+            read = jnp.dot(
+                head_query,
+                updated,
+                precision=lax.Precision.HIGHEST,
+                preferred_element_type=jnp.float32,
+            )
+            readout_v[s : s + 1, h * value_width : (h + 1) * value_width] = read[s : s + 1, :]
+    store = pltpu.make_async_copy(memory_v, memory_next, store_sem)
+    for h in range(heads_local):
+        span = slice(h * value_width, (h + 1) * value_width)
+        readout = readout_v[:, span]
+        normalized = readout * lax.rsqrt(
+            jnp.mean(readout * readout, axis=-1, keepdims=True) + epsilon
+        )
+        gated = (
+            normalized * head_gain[:, span].astype(jnp.float32) / (1.0 + jnp.exp(-outgate[:, span]))
+        )
+        mixed_send[:, span] = gated.astype(jnp.bfloat16).astype(jnp.float32)[0:seq_local, :]
+    store.start()
+    for step in range(1, kv_count):
+        kv_copy(mixed_send, mixed_land, 1, (my_kv + step) % kv_count).start()
+    mixed_land[my_kv] = mixed_send[...]
+    loads[10].wait()
+    for step in range(1, kv_count):
+        kv_arrived(mixed_land, 1, (my_kv + step) % kv_count)
+    for k in range(kv_count):
+        mixed_all[k * seq_local : (k + 1) * seq_local, :] = mixed_land[k]
+    mix_terms = jnp.dot(
+        mixed_all[...].astype(jnp.bfloat16), mixout_w[...], preferred_element_type=jnp.float32
+    ).astype(jnp.bfloat16)
+    for t in range(tp_count):
+        mix_send[t] = mix_terms[:, t * chunk : (t + 1) * chunk]
+    for step in range(1, tp_count):
+        peer = (my_tp + step) % tp_count
+        tp_copy(mix_send.at[peer], mix_land, 1, peer).start()
+    branch = mix_send[my_tp].astype(jnp.float32)
+    for step in range(1, tp_count):
+        peer = (my_tp + step) % tp_count
+        tp_arrived(mix_land, 1, peer)
+        branch = branch + mix_land[peer].astype(jnp.float32)
+    after_v[...] = (first.astype(jnp.float32) + branch).astype(jnp.bfloat16)
+    layer_out[...] = half(
+        after_v, second_gain, gate_b, up_b, down_b, gathered_b, parts_b, landed_b, 2, ready_b
+    )
+
+    sent_all(lambda peer: tokens, gathered_a, 0)
+    sent_all(lambda peer: parts_a.at[peer], landed_a, 1)
+    sent_all(lambda peer: after_v, gathered_b, 2)
+    sent_all(lambda peer: parts_b.at[peer], landed_b, 3)
+    for step in range(1, tp_count):
+        peer = (my_tp + step) % tp_count
+        tp_copy(first_v, block_v, 0, peer).wait_send()
+        tp_copy(mix_send.at[peer], mix_land, 1, peer).wait_send()
+    for step in range(1, kv_count):
+        peer = (my_kv + step) % kv_count
+        kv_copy(proj_send.at[peer], proj_land, 0, peer).wait_send()
+        kv_copy(mixed_send, mixed_land, 1, peer).wait_send()
+    store.wait()
+
+
+def fused_on_device(
+    kv_count,
+    tp_count,
+    tokens,
+    first_gain,
+    first_gate,
+    first_up,
+    first_down,
+    mix_gain,
+    query_weight,
+    key_weight,
+    value_weight,
+    outgate_weight,
+    ingate_weight,
+    forget_weight,
+    forget_bias,
+    head_gain,
+    mixout_weight,
+    memory,
+    stabilizer,
+    second_gain,
+    second_gate,
+    second_up,
+    second_down,
+):
+    total = kv_count * tp_count
+    rows, chunk = tokens.shape
+    seq_local = memory.shape[0]
+    width = sum(w.shape[1] for w in (query_weight, key_weight, value_weight, outgate_weight)) + 384
+    mixed_width = outgate_weight.shape[1]
+    held_rows = max(8, seq_local)
+
+    def like(array):
+        return pltpu.VMEM(array.shape, array.dtype)
+
+    exchange = pltpu.VMEM((total, rows, chunk), jnp.bfloat16)
+    tile = pltpu.VMEM((rows, chunk), jnp.bfloat16)
+    tp_tiles = pltpu.VMEM((tp_count, rows, chunk), jnp.bfloat16)
+    vmem = pl.BlockSpec(memory_space=pltpu.VMEM)
+    hbm = pl.BlockSpec(memory_space=pl.ANY)
+    return pl.pallas_call(
+        functools.partial(fused_kernel, kv_count, tp_count),
+        out_shape=(
+            jax.ShapeDtypeStruct(tokens.shape, jnp.bfloat16),
+            jax.ShapeDtypeStruct(memory.shape, memory.dtype),
+            jax.ShapeDtypeStruct(stabilizer.shape, stabilizer.dtype),
+        ),
+        in_specs=[vmem] * 7 + [hbm] * 14,
+        out_specs=(vmem, hbm, vmem),
+        scratch_shapes=[
+            like(first_gate),
+            like(first_up),
+            like(first_down),
+            like(second_gate),
+            like(second_up),
+            like(second_down),
+            like(query_weight),
+            like(key_weight),
+            like(value_weight),
+            like(outgate_weight),
+            like(ingate_weight),
+            like(forget_weight),
+            like(mixout_weight),
+            like(memory),
+            exchange,
+            exchange,
+            exchange,
+            exchange,
+            exchange,
+            exchange,
+            tile,
+            tp_tiles,
+            pltpu.VMEM((kv_count, seq_local, width), jnp.float32),
+            pltpu.VMEM((kv_count, seq_local, width), jnp.float32),
+            pltpu.VMEM((held_rows, width), jnp.float32),
+            pltpu.VMEM((held_rows, mixed_width), jnp.float32),
+            pltpu.VMEM((seq_local, mixed_width), jnp.float32),
+            pltpu.VMEM((kv_count, seq_local, mixed_width), jnp.float32),
+            pltpu.VMEM((rows, mixed_width), jnp.float32),
+            tp_tiles,
+            tp_tiles,
+            tile,
+            pltpu.SemaphoreType.DMA((14,)),
+            pltpu.SemaphoreType.DMA,
+            pltpu.SemaphoreType.DMA((4, total)),
+            pltpu.SemaphoreType.DMA((4, total)),
+            pltpu.SemaphoreType.DMA((2, tp_count)),
+            pltpu.SemaphoreType.DMA((2, tp_count)),
+            pltpu.SemaphoreType.DMA((2, kv_count)),
+            pltpu.SemaphoreType.DMA((2, kv_count)),
+        ],
+        compiler_params=pltpu.CompilerParams(
+            collective_id=0, has_side_effects=True, vmem_limit_bytes=60 * 1024 * 1024
+        ),
+    )(
+        tokens,
+        first_gain[None, :],
+        mix_gain[None, :],
+        second_gain[None, :],
+        head_gain[None, :],
+        forget_bias[None, :],
+        stabilizer,
+        first_gate,
+        first_up,
+        first_down,
+        query_weight,
+        key_weight,
+        value_weight,
+        outgate_weight,
+        ingate_weight,
+        forget_weight,
+        mixout_weight,
+        memory,
+        second_gate,
+        second_up,
+        second_down,
+    )
+
+
+def choose(kv_count, tp_count, *arrays):
+    if arrays[0].shape[1] % 128 == 0:
+        return fused_on_device(kv_count, tp_count, *arrays)
+    return on_device(*arrays)
+
+
 def solution(mesh):
     in_specs = (
         P(None, ("kv", "tp")),
@@ -160,5 +729,7 @@
     )
     out_specs = (P(None, ("kv", "tp")), P("kv", "tp", None, None), P("kv", "tp"))
     return jax.shard_map(
-        on_device, mesh=mesh, in_specs=in_specs, out_specs=out_specs, check_vma=False
-    )
+        functools.partial(choose, mesh.shape["kv"], mesh.shape["tp"]),
+        mesh=mesh,
+        in_specs=in_specs, out_specs=out_specs, check_vma=False
+    )

time: 593 us -> 95.8 us (0.16)
  waiting for transfers between devices: 418 us -> 0 us
  blocking collectives: 121 us -> 0 us
  Pallas kernels: 0 us -> 64.5 us
  local copies, waits for them, and re-layouts: 4.05 us -> 29.5 us
  matrix products: 24.9 us -> 0 us
  between operations: 14.6 us -> 0.65 us
  other arithmetic: 9.58 us -> 0 us
    reduce_scatter x2 -> x0, waiting for transfers between devices: 261 us -> none  [half_mlp(): lax.psum_scatter(lax.dot_general(down_weight, hidden, (((0,), (1,)), ((),...]
    unnamed x8 -> x0, waiting for transfers between devices: 156 us -> none
    all_gather x4 -> x0, blocking collectives: 121 us -> none  [the longest x2 85.5 us: half_mlp(): lax.all_gather(tokens, ('kv', 'tp'), axis=1, tiled=True)]
    pallas_call x0 -> x1, Pallas kernels: none -> 64.5 us  [fused_on_device(): pl.pallas_call(functools.partial(fused_kernel, kv_count, tp_count), out_s...]
    dot_general x12 -> x0, matrix products: 24.9 us -> none  [the longest x8 14.1 us: fold_columns(): jnp.dot(normed, matrix, preferred_element_type=jnp.float32)]
    unnamed x29 -> x13, local copies, waits for them, and re-layouts: 3.97 us -> 23.1 us
  transfers between devices with their start and end apart: 5 -> 0, of which waited for: 5 -> 0; matrix products, arithmetic and copies ran while one was open for 1% -> 0% of each run, Pallas kernels for 0% -> 0%
where the time goes in v1:
time: 95.8 us; the launch traced here: 94.7 us
  Pallas kernels  64.5 us (67%)
  local copies, waits for them, and re-layouts  29.5 us (31%)
    pallas_call x1, Pallas kernels, fused_on_device(): pl.pallas_call(functools.partial(fused_kernel, kv_count, tp_count), out_s...  64.5 us
    unnamed x13, local copies, waits for them, and re-layouts  23.1 us

profile of v1, /device:TPU:0, one launch (start us, length us, event | category | flops | bytes accessed | tf_op | source)
XLA Modules:
  0.0 94.7 jit_solution(17308291372453956376)
XLA Ops:
  0.6 1.3 %broadcast_in_dim.18.head_gain = bf16[1,512]{1,0:T(2,128)(2,1)} reshape(bf16[512]{0:T(512)(128)(2,1)} %param.34) | data formatting | bytes 2048 | tf_op jit(solution)/shard_map/broadcast_in_dim | solution.py:680
  1.9 1.3 %copy.24.stabilizer = f32[4,2]{1,0:T(4,128)} copy(f32[4,2]{0,1:T(2,128)} %param.37) | data formatting | bytes 64 | tf_op args[16]
  3.2 1.3 %broadcast_in_dim.15.first_gain = bf16[1,4096]{1,0:T(2,128)(2,1)} reshape(bf16[4096]{0:T(1024)(128)(2,1)} %param.22) | data formatting | bytes 16384 | tf_op jit(solution)/shard_map/broadcast_in_dim | solution.py:677
  4.5 1.3 %broadcast_in_dim.16.mix_gain = bf16[1,4096]{1,0:T(2,128)(2,1)} reshape(bf16[4096]{0:T(1024)(128)(2,1)} %param.26) | data formatting | bytes 16384 | tf_op jit(solution)/shard_map/broadcast_in_dim | solution.py:678
  5.8 1.3 %broadcast_in_dim.17.second_gain = bf16[1,4096]{1,0:T(2,128)(2,1)} reshape(bf16[4096]{0:T(1024)(128)(2,1)} %param.38) | data formatting | bytes 16384 | tf_op jit(solution)/shard_map/broadcast_in_dim | solution.py:679
  7.1 1.5 %copy.27.ingate_weight = bf16[512,8]{1,0:T(8,128)(2,1)} copy(bf16[512,8]{0,1:T(8,128)(2,1)} %param.31) | data formatting | bytes 16384 | tf_op args[10]
  8.6 1.5 %copy.28.forget_weight = bf16[512,8]{1,0:T(8,128)(2,1)} copy(bf16[512,8]{0,1:T(8,128)(2,1)} %param.32) | data formatting | bytes 16384 | tf_op args[11]
  10.1 0.0 copy-start
  10.1 4.8 %copy.25.first_gate = bf16[4096,352]{1,0:T(8,128)(2,1)} copy(bf16[4096,352]{0,1:T(8,128)(2,1)} %param.23) | data formatting | bytes 5767168 | tf_op args[2]
  14.9 0.0 copy-done
  14.9 2.8 %copy.26.first_up = bf16[4096,352]{1,0:T(8,128)(2,1)} copy(bf16[4096,352]{0,1:T(8,128)(2,1)S(1)} %copy-done) | data formatting | bytes 5767168 | tf_op args[3]
  17.7 0.0 copy-start.1
  17.7 4.8 %copy.29.second_gate = bf16[4096,352]{1,0:T(8,128)(2,1)} copy(bf16[4096,352]{0,1:T(8,128)(2,1)} %param.39) | data formatting | bytes 5767168 | tf_op args[18]
  22.5 0.0 copy-done.1
  22.5 2.8 %copy.30.second_up = bf16[4096,352]{1,0:T(8,128)(2,1)} copy(bf16[4096,352]{0,1:T(8,128)(2,1)S(1)} %copy-done.1) | data formatting | bytes 5767168 | tf_op args[19]
  25.3 64.5 %shard_map.220 = (bf16[32,128]{1,0:T(8,128)(2,1)}, f32[4,2,128,256]{3,2,1,0:T(8,128)}, f32[4,2]{1,0:T(4,128)}) custom-call(bf16[32,128]{1,0:T(8,128)(2,1)} %tokens.1, bf16[1,4096]{1,0:T(2,128)(2,1)} %broadcast_in_dim.15.first_gain, bf16[1,4096]{1,0:T(2,128)(2,1)} %broadcast_in_dim.16.mix_gain, bf16[1,4096]{1,0:T(2,128)(2,1)} %broadcast_in_dim.17.second_gain, ...), custom_call_target="tpu_custom_call" | custom-call | tf_op jit(solution)/shard_map/pallas_call | solution.py:621
  89.8 1.3 %copy.31 = f32[4,2]{0,1:T(2,128)} copy(f32[4,2]{1,0:T(4,128)} %get-tuple-element.5) | data formatting | bytes 64 | tf_op jit(solution)/shard_map/pallas_call | solution.py:621
  91.1 1.3 %copy.34 = bf16[32,128]{1,0:T(8,128)(2,1)} copy(bf16[32,128]{1,0:T(8,128)(2,1)} %get-tuple-element.9) | data formatting | bytes 16384
  92.4 2.3 %copy.35 = f32[4,2,128,256]{3,2,1,0:T(8,128)} copy(f32[4,2,128,256]{3,2,1,0:T(8,128)} %get-tuple-element.10) | data formatting | bytes 2097152
Async XLA Ops:
  10.1 4.8 %copy-start = (bf16[4096,352]{0,1:T(8,128)(2,1)S(1)}, bf16[4096,352]{0,1:T(8,128)(2,1)}, u32[]{:S(2)}) copy-start(bf16[4096,352]{0,1:T(8,128)(2,1)} %param.24) | copy-start | bytes 8650756
  17.7 4.8 %copy-start.1 = (bf16[4096,352]{0,1:T(8,128)(2,1)S(1)}, bf16[4096,352]{0,1:T(8,128)(2,1)}, u32[]{:S(2)}) copy-start(bf16[4096,352]{0,1:T(8,128)(2,1)} %param.40) | copy-start | bytes 8650756

commit v2 on v1

--- a/solution.py
+++ b/solution.py
@@ -207,6 +207,7 @@
     kv_recv,
 ):
     total = kv_count * tp_count
+    wide_dims = (((1,), (1,)), ((), ()))
     my_kv = lax.axis_index("kv")
     my_tp = lax.axis_index("tp")
     me = my_kv * tp_count + my_tp
@@ -264,32 +265,53 @@
             device_id_type=pl.DeviceIdType.MESH,
         )
 
+    partner_tp = my_tp + 1 - 2 * (my_tp % 2)
+
+    def twin(peer):
+        return peer + 1 - 2 * (peer % 2)
+
+    def direct(source, target, phase, peer):
+        return send(
+            source,
+            target.at[me],
+            all_send.at[phase, peer],
+            all_recv.at[phase, me],
+            peer // tp_count,
+            peer % tp_count,
+        )
+
+    def forward(source, target, phase, peer):
+        return send(
+            source,
+            target.at[peer],
+            all_send.at[phase, twin(peer)],
+            all_recv.at[phase, peer],
+            my_kv,
+            partner_tp,
+        )
+
     def share_all(source, target, phase):
         def step_of(step, carry):
-            peer = (me + step) % total
-            send(
-                source,
-                target.at[me],
-                all_send.at[phase, peer],
-                all_recv.at[phase, me],
-                peer // tp_count,
-                peer % tp_count,
-            ).start()
+            direct(source, target, phase, (me + 2 * step) % total).start()
             return carry
 
-        lax.fori_loop(1, total, step_of, 0)
-
-    def sent_all(source_of, target, phase):
+        forward(source, target, phase, me).start()
+        lax.fori_loop(1, total // 2, step_of, 0)
+
+    def shared_all(source, target, phase):
+        def step_of(step, carry):
+            peer = (me + 2 * step) % total
+            direct(source, target, phase, peer).wait_send()
+            forward(target.at[peer], target, phase, peer).wait_send()
+            return carry
+
+        forward(source, target, phase, me).wait_send()
+        lax.fori_loop(1, total // 2, step_of, 0)
+
+    def sent_all(source, target, phase):
         def step_of(step, carry):
             peer = (me + step) % total
-            send(
-                source_of(peer),
-                target.at[me],
-                all_send.at[phase, peer],
-                all_recv.at[phase, me],
-                peer // tp_count,
-                peer % tp_count,
-            ).wait_send()
+            direct(source.at[peer], target, phase, peer).wait_send()
             return carry
 
         lax.fori_loop(1, total, step_of, 0)
@@ -308,17 +330,18 @@
         share_all(own, gathered, phase)
         gathered[me] = own[...]
         ready(0)
-        hidden_units = gate_w.shape[1]
+        hidden_units = gate_w.shape[0]
 
         def group_of(step, carry):
             gate_sum, up_sum, squares = carry
             group = (my_kv + step) % kv_count
-            for t in range(tp_count):
-                peer = group * tp_count + t
-
-                @pl.when(peer != me)
-                def _():
-                    arrived(gathered, phase, peer)
+
+            @pl.when(step < kv_count - 1)
+            def _():
+                relay((my_kv + step + 1) % kv_count)
+
+            for pair in range(tp_count // 2):
+                arrived(gathered, phase, group * tp_count + 2 * pair + 1 - my_tp % 2)
 
             wide = jnp.concatenate(
                 [gathered[group * tp_count + t].astype(jnp.float32) for t in range(tp_count)],
@@ -326,14 +349,24 @@
             )
             start = pl.multiple_of(group * block, block)
             normed = (wide * gain[:, pl.ds(start, block)].astype(jnp.float32)).astype(jnp.bfloat16)
-            gate_sum = gate_sum + jnp.dot(
-                normed, gate_w[pl.ds(start, block), :], preferred_element_type=jnp.float32
+            gate_sum = gate_sum + lax.dot_general(
+                normed, gate_w[:, pl.ds(start, block)], wide_dims, preferred_element_type=jnp.float32
             )
-            up_sum = up_sum + jnp.dot(
-                normed, up_w[pl.ds(start, block), :], preferred_element_type=jnp.float32
+            up_sum = up_sum + lax.dot_general(
+                normed, up_w[:, pl.ds(start, block)], wide_dims, preferred_element_type=jnp.float32
             )
             return gate_sum, up_sum, squares + jnp.sum(wide * wide, axis=1, keepdims=True)
 
+        def relay(group):
+            for pair in range(tp_count // 2):
+                peer = group * tp_count + 2 * pair + my_tp % 2
+
+                @pl.when(peer != me)
+                def _():
+                    arrived(gathered, phase, peer)
+                    forward(gathered.at[peer], gathered, phase, peer).start()
+
+        relay(my_kv)
         zero = jnp.zeros((rows, hidden_units), jnp.float32)
         gate_sum, up_sum, squares = lax.fori_loop(
             0, kv_count, group_of, (zero, zero, jnp.zeros((rows, 1), jnp.float32))
@@ -349,14 +382,7 @@
 
                 @pl.when(peer != me)
                 def _():
-                    send(
-                        parts.at[peer],
-                        landed.at[me],
-                        all_send.at[phase + 1, peer],
-                        all_recv.at[phase + 1, me],
-                        group,
-                        t,
-                    ).start()
+                    direct(parts.at[peer], landed, phase + 1, peer).start()
 
         def down_of(step, carry):
             group = (my_kv + 1 + step) % kv_count
@@ -453,13 +479,18 @@
         offsets.append(offsets[-1] + weight.shape[1])
     edge = offsets[-1]
     lane = 128
-    head_count = ingate_w.shape[1]
+    head_count = ingate_w.shape[0]
     pieces = [
         (offset, jnp.dot(normed, weight[...], preferred_element_type=jnp.float32))
         for offset, weight in zip(
-            offsets[:4] + [edge, edge + lane],
-            (query_w, key_w, value_w, outgate_w, ingate_w, forget_w),
-        )
+            offsets, (query_w, key_w, value_w, outgate_w)
+        )
+    ] + [
+        (
+            edge + n * lane,
+            lax.dot_general(normed, weight[...], wide_dims, preferred_element_type=jnp.float32),
+        )
+        for n, weight in enumerate((ingate_w, forget_w))
     ]
     squares = jnp.broadcast_to(jnp.sum(wide * wide, axis=1, keepdims=True), (rows, lane))
     pieces.append((edge + 2 * lane, squares))
@@ -563,10 +594,10 @@
         after_v, second_gain, gate_b, up_b, down_b, gathered_b, parts_b, landed_b, 2, ready_b
     )
 
-    sent_all(lambda peer: tokens, gathered_a, 0)
-    sent_all(lambda peer: parts_a.at[peer], landed_a, 1)
-    sent_all(lambda peer: after_v, gathered_b, 2)
-    sent_all(lambda peer: parts_b.at[peer], landed_b, 3)
+    shared_all(tokens, gathered_a, 0)
+    sent_all(parts_a, landed_a, 1)
+    shared_all(after_v, gathered_b, 2)
+    sent_all(parts_b, landed_b, 3)
     for step in range(1, tp_count):
         peer = (my_tp + step) % tp_count
         tp_copy(first_v, block_v, 0, peer).wait_send()
@@ -606,6 +637,13 @@
     total = kv_count * tp_count
     rows, chunk = tokens.shape
     seq_local = memory.shape[0]
+    first_gate, first_up, second_gate, second_up = (
+        first_gate.T,
+        first_up.T,
+        second_gate.T,
+        second_up.T,
+    )
+    ingate_weight, forget_weight = ingate_weight.T, forget_weight.T
     width = sum(w.shape[1] for w in (query_weight, key_weight, value_weight, outgate_weight)) + 384
     mixed_width = outgate_weight.shape[1]
     held_rows = max(8, seq_local)
@@ -698,7 +736,7 @@
 
 
 def choose(kv_count, tp_count, *arrays):
-    if arrays[0].shape[1] % 128 == 0:
+    if arrays[0].shape[1] % 128 == 0 and tp_count % 2 == 0:
         return fused_on_device(kv_count, tp_count, *arrays)
     return on_device(*arrays)
 

time: 95.8 us -> 79.1 us (0.83)
  local copies, waits for them, and re-layouts: 29.5 us -> 11.4 us
  Pallas kernels: 64.5 us -> 66.6 us
    unnamed x13 -> x3, local copies, waits for them, and re-layouts: 23.1 us -> 4.91 us
    pallas_call x1, Pallas kernels: 64.5 us -> 66.6 us  [fused_on_device(): pl.pallas_call(functools.partial(fused_kernel, kv_count, tp_count), out_s...]
where the time goes in v2:
time: 79.1 us; the launch traced here: 78.6 us
  Pallas kernels  66.6 us (84%)
  local copies, waits for them, and re-layouts  11.4 us (14%)
    pallas_call x1, Pallas kernels, fused_on_device(): pl.pallas_call(functools.partial(fused_kernel, kv_count, tp_count), out_s...  66.6 us
    unnamed x3, local copies, waits for them, and re-layouts  4.91 us

profile of v2, /device:TPU:0, one launch (start us, length us, event | category | flops | bytes accessed | tf_op | source)
XLA Modules:
  0.0 78.6 jit_solution(16269671576215766918)
XLA Ops:
  0.6 1.3 %broadcast_in_dim.18.head_gain = bf16[1,512]{1,0:T(2,128)(2,1)} reshape(bf16[512]{0:T(512)(128)(2,1)} %param.34) | data formatting | bytes 2048 | tf_op jit(solution)/shard_map/broadcast_in_dim | solution.py:718
  1.9 1.3 %copy.24.stabilizer = f32[4,2]{1,0:T(4,128)} copy(f32[4,2]{0,1:T(2,128)} %param.37) | data formatting | bytes 64 | tf_op args[16]
  3.2 1.3 %broadcast_in_dim.15.first_gain = bf16[1,4096]{1,0:T(2,128)(2,1)} reshape(bf16[4096]{0:T(1024)(128)(2,1)} %param.22) | data formatting | bytes 16384 | tf_op jit(solution)/shard_map/broadcast_in_dim | solution.py:715
  4.5 1.3 %broadcast_in_dim.16.mix_gain = bf16[1,4096]{1,0:T(2,128)(2,1)} reshape(bf16[4096]{0:T(1024)(128)(2,1)} %param.26) | data formatting | bytes 16384 | tf_op jit(solution)/shard_map/broadcast_in_dim | solution.py:716
  5.9 1.3 %broadcast_in_dim.17.second_gain = bf16[1,4096]{1,0:T(2,128)(2,1)} reshape(bf16[4096]{0:T(1024)(128)(2,1)} %param.38) | data formatting | bytes 16384 | tf_op jit(solution)/shard_map/broadcast_in_dim | solution.py:717
  7.2 66.6 %shard_map.220 = (bf16[32,128]{1,0:T(8,128)(2,1)}, f32[4,2,128,256]{3,2,1,0:T(8,128)}, f32[4,2]{1,0:T(4,128)}) custom-call(bf16[32,128]{1,0:T(8,128)(2,1)} %tokens.1, bf16[1,4096]{1,0:T(2,128)(2,1)} %broadcast_in_dim.15.first_gain, bf16[1,4096]{1,0:T(2,128)(2,1)} %broadcast_in_dim.16.mix_gain, bf16[1,4096]{1,0:T(2,128)(2,1)} %broadcast_in_dim.17.second_gain, ...), custom_call_target="tpu_custom_call" | custom-call | tf_op jit(solution)/shard_map/pallas_call | solution.py:659
  73.7 1.3 %copy.25 = f32[4,2]{0,1:T(2,128)} copy(f32[4,2]{1,0:T(4,128)} %get-tuple-element.5) | data formatting | bytes 64 | tf_op jit(solution)/shard_map/pallas_call | solution.py:659
  75.0 1.3 %copy.28 = bf16[32,128]{1,0:T(8,128)(2,1)} copy(bf16[32,128]{1,0:T(8,128)(2,1)} %get-tuple-element.9) | data formatting | bytes 16384
  76.3 2.3 %copy.29 = f32[4,2,128,256]{3,2,1,0:T(8,128)} copy(f32[4,2,128,256]{3,2,1,0:T(8,128)} %get-tuple-element.10) | data formatting | bytes 2097152

commit v3 on v2

--- a/solution.py
+++ b/solution.py
@@ -348,7 +348,7 @@
                 axis=1,
             )
             start = pl.multiple_of(group * block, block)
-            normed = (wide * gain[:, pl.ds(start, block)].astype(jnp.float32)).astype(jnp.bfloat16)
+            normed = (wide * gain[pl.ds(start, block)].astype(jnp.float32)[None, :]).astype(jnp.bfloat16)
             gate_sum = gate_sum + lax.dot_general(
                 normed, gate_w[:, pl.ds(start, block)], wide_dims, preferred_element_type=jnp.float32
             )
@@ -473,7 +473,7 @@
         tp_arrived(block_v, 0, (my_tp + step) % tp_count)
     wide = jnp.concatenate([block_v[t].astype(jnp.float32) for t in range(tp_count)], axis=1)
     start = pl.multiple_of(my_kv * block, block)
-    normed = (wide * mix_gain[:, pl.ds(start, block)].astype(jnp.float32)).astype(jnp.bfloat16)
+    normed = (wide * mix_gain[pl.ds(start, block)].astype(jnp.float32)[None, :]).astype(jnp.bfloat16)
     offsets = [0]
     for weight in (query_w, key_w, value_w, outgate_w):
         offsets.append(offsets[-1] + weight.shape[1])
@@ -526,11 +526,24 @@
     ingate = (factor * ingate)[0:seq_local]
     forget = (factor * forget)[0:seq_local] + forget_bias[...]
     log_forget = jnp.minimum(forget, 0.0) - jnp.log1p(jnp.exp(-jnp.abs(forget)))
-    shifted = log_forget + stabilizer[...]
+    diagonal = lax.broadcasted_iota(jnp.int32, (seq_local, seq_local), 0) == (
+        lax.broadcasted_iota(jnp.int32, (seq_local, seq_local), 1)
+    )
+    head_lane = lax.broadcasted_iota(jnp.int32, (seq_local, heads_local), 1)
+    scale_now = jnp.zeros((seq_local, heads_local), jnp.float32)
+    for h in range(heads_local):
+        column = jnp.sum(
+            jnp.where(diagonal, stabilizer[h : h + 1, :], 0.0), axis=1, keepdims=True
+        )
+        scale_now = jnp.where(head_lane == h, column, scale_now)
+    shifted = log_forget + scale_now
     ceiling = jnp.maximum(shifted, ingate)
     retain = jnp.exp(shifted - ceiling)
     admission = jnp.exp(ingate - ceiling) * key_width ** (-0.5)
-    ceiling_out[...] = ceiling
+    for h in range(heads_local):
+        ceiling_out[h : h + 1, :] = jnp.sum(
+            jnp.where(diagonal, ceiling[:, h : h + 1], 0.0), axis=0, keepdims=True
+        )
     row_index = lax.broadcasted_iota(jnp.int32, (reduced.shape[0], key_width), 0)
     stores = []
     for h in range(heads_local):
@@ -564,7 +577,7 @@
             jnp.mean(readout * readout, axis=-1, keepdims=True) + epsilon
         )
         gated = (
-            normalized * head_gain[:, span].astype(jnp.float32) / (1.0 + jnp.exp(-outgate[:, span]))
+            normalized * head_gain[span].astype(jnp.float32)[None, :] / (1.0 + jnp.exp(-outgate[:, span]))
         )
         mixed_send[:, span] = gated.astype(jnp.bfloat16).astype(jnp.float32)[0:seq_local, :]
     store.start()
@@ -656,12 +669,12 @@
     tp_tiles = pltpu.VMEM((tp_count, rows, chunk), jnp.bfloat16)
     vmem = pl.BlockSpec(memory_space=pltpu.VMEM)
     hbm = pl.BlockSpec(memory_space=pl.ANY)
-    return pl.pallas_call(
+    layer_out, memory_next, ceiling = pl.pallas_call(
         functools.partial(fused_kernel, kv_count, tp_count),
         out_shape=(
             jax.ShapeDtypeStruct(tokens.shape, jnp.bfloat16),
             jax.ShapeDtypeStruct(memory.shape, memory.dtype),
-            jax.ShapeDtypeStruct(stabilizer.shape, stabilizer.dtype),
+            jax.ShapeDtypeStruct(stabilizer.shape[::-1], stabilizer.dtype),
         ),
         in_specs=[vmem] * 7 + [hbm] * 14,
         out_specs=(vmem, hbm, vmem),
@@ -712,12 +725,12 @@
         ),
     )(
         tokens,
-        first_gain[None, :],
-        mix_gain[None, :],
-        second_gain[None, :],
-        head_gain[None, :],
+        first_gain,
+        mix_gain,
+        second_gain,
+        head_gain,
         forget_bias[None, :],
-        stabilizer,
+        stabilizer.T,
         first_gate,
         first_up,
         first_down,
@@ -733,6 +746,7 @@
         second_up,
         second_down,
     )
+    return layer_out, memory_next, ceiling.T
 
 
 def choose(kv_count, tp_count, *arrays):

time: 79.1 us -> 72.3 us (0.914)
  local copies, waits for them, and re-layouts: 11.4 us -> 4.78 us
    broadcast_in_dim x4 -> x0, local copies, waits for them, and re-layouts: 5.18 us -> none  [the longest x1 1.31 us: fused_on_device(): first_gain[None, :]]
    pallas_call x1 -> x0, local copies, waits for them, and re-layouts: 1.33 us -> none  [fused_on_device(): pl.pallas_call(functools.partial(fused_kernel, kv_count, tp_count), out_s...]
where the time goes in v3:
time: 72.3 us; the launch traced here: 72.1 us
  Pallas kernels  66.6 us (92%)
  local copies, waits for them, and re-layouts  4.78 us (7%)
    pallas_call x1, Pallas kernels, fused_on_device(): pl.pallas_call(functools.partial(fused_kernel, kv_count, tp_count), out_s...  66.6 us
    unnamed x3, local copies, waits for them, and re-layouts  4.78 us

profile of v3, /device:TPU:0, one launch (start us, length us, event | category | flops | bytes accessed | tf_op | source)
XLA Modules:
  0.0 72.1 jit_solution(16977441648014827683)
XLA Ops:
  0.6 66.6 %shard_map.220 = (bf16[32,128]{1,0:T(8,128)(2,1)}, f32[4,2,128,256]{3,2,1,0:T(8,128)}, f32[2,4]{1,0:T(2,128)}) custom-call(bf16[32,128]{1,0:T(8,128)(2,1)} %tokens.1, bf16[4096]{0:T(1024)(128)(2,1)} %first_gain.1, bf16[4096]{0:T(1024)(128)(2,1)} %mix_gain.1, bf16[4096]{0:T(1024)(128)(2,1)} %second_gain.1, bf16[512]{0:T(512)(128)(2,1)} %head_gain.1, ...), custom_call_target="tpu_custom_call" | custom-call | tf_op jit(solution)/shard_map/pallas_call | solution.py:672
  67.3 1.3 %copy.27 = bf16[32,128]{1,0:T(8,128)(2,1)} copy(bf16[32,128]{1,0:T(8,128)(2,1)} %get-tuple-element.12) | data formatting | bytes 16384
  68.6 2.3 %copy.28 = f32[4,2,128,256]{3,2,1,0:T(8,128)} copy(f32[4,2,128,256]{3,2,1,0:T(8,128)} %get-tuple-element.13) | data formatting | bytes 2097152
  70.8 1.2 %copy.29 = f32[4,2]{0,1:T(2,128)} copy(f32[4,2]{0,1:T(2,128)} %bitcast.16) | data formatting | bytes 64
